TPU v7x, 32 devices: a whole 2x2x4 slice. The times are simulated.
32 devices in a mesh: sp: 4 (over y, x), tp: 8 (over z, core).
Axes of the slice: x: 2, y: 2, z: 4, core: 2. Of those that a mesh axis runs over, the one named last changes fastest.
Arguments:
- skip_stream_entry: bfloat16 [2048, 2048], P(('sp', 'tp')), may hold values from -6 to 6
- result_switch_mapped: bfloat16 [2048, 4096], P('sp', 'tp'), may hold values from -6 to 6
- channel_feed_mapped: bfloat16 [2048, 4096], P('sp', 'tp'), may hold values from -6 to 6
- write_coefficient_mapped: bfloat16 [2048, 2048], P('sp', 'tp'), may hold values from -6 to 6
- emission_coefficient_mapped: bfloat16 [2048, 2048], P('sp', 'tp'), may hold values from -6 to 6
- channel_feed_taps: bfloat16 [5, 4096], P(None, 'tp'), may hold values from -2.5 to 2.5
- write_coefficient_taps: bfloat16 [5, 2048], P(None, 'tp'), may hold values from -2.5 to 2.5
- emission_coefficient_taps: bfloat16 [5, 2048], P(None, 'tp'), may hold values from -2.5 to 2.5
- raw_increments: bfloat16 [2, 64, 2048], P(None, 'tp', 'sp'), may hold values from -6 to 6
- channel_log_fade_speed: float32 [2, 64], P(None, 'tp'), may hold values from -20 to 0
- extra_log_fade: float32 [2, 64, 2048], P(None, 'tp', 'sp'), may hold values from -1 to 0
- cluster_scaling_factor: float32 [4096], P('tp'), may hold values from 0.1 to 1.9
- blend_result_matrix: bfloat16 [4096, 2048], P('tp'), may hold values from -0.09375 to 0.09375
- routing_scaling_factor: float32 [2048], replicated, may hold values from 0.1 to 1.9
- specialist_switch_matrix: bfloat16 [8, 2048, 4096], P('sp', None, 'tp'), may hold values from -0.125 to 0.125
- specialist_widen_matrix: bfloat16 [8, 2048, 4096], P('sp', None, 'tp'), may hold values from -0.125 to 0.125
- specialist_contract_matrix: bfloat16 [8, 4096, 2048], P('sp', 'tp'), may hold values from -0.1875 to 0.1875
- picked_specialists: int32 [2048, 2], P(('sp', 'tp')), may hold values from 0 to 7, all different within a row; in each aligned block of 64 rows (0 to 63, 64 to 127, ...) at most 24 rows name the same one
- router_affinities: float32 [2048, 2], P(('sp', 'tp')), may hold values from 0.1 to 1
Outputs:
- result: bfloat16 [2048, 2048], P(('sp', 'tp'))
Inputs may be any that keep to these rules, and one draw needn't show every extreme that they name: `picked_specialists`: each row names 2 different experts. Within the rows of one device (aligned blocks of 64 rows) no expert is named more than 24 times, a bound that some block reaches.
All inputs are finite; a program needn't handle non-finite values.
Results may differ from a plain program's by a relative error of at most 0.02.
Values may be sent and summed in bfloat16 or wider, within the bound.
A program may use at most 64 MiB of HBM per device.

v0:
```python
import jax
import jax.numpy as jnp
from jax import lax
from jax.sharding import PartitionSpec as P

WIDTH = 2048
HEAD_DIM = 64
GROUPS = 16
STATE = 128
CONV_W = 5
BLOCK = 128
TOP = 2
INNER = 4096


EPSILON = 1e-06
HIGHEST_MODE = lax.Precision.HIGHEST


def with_halo(block, sides, width):
    for axis, dim in sides:
        count = lax.axis_size(axis)
        forward = [(i, i + 1) for i in range(count - 1)]
        backward = [(target, source) for source, target in forward]
        low = lax.ppermute(
            lax.slice_in_dim(block, block.shape[dim] - width, None, axis=dim), axis, forward
        )
        high = lax.ppermute(lax.slice_in_dim(block, 0, width, axis=dim), axis, backward)
        block = jnp.concatenate([low, block, high], axis=dim)
    return block


def prefix(shard, axis, combine, identity, reverse):
    peers, here = (lax.axis_size(axis), lax.axis_index(axis))
    everything = jax.tree.map(
        lambda part, kind: lax.all_gather(part.astype(kind), axis),
        shard,
        (jnp.bfloat16, jnp.bfloat16),
    )
    start = jax.tree.map(
        lambda part, zero: jnp.broadcast_to(jnp.asarray(zero, part.dtype), part.shape),
        shard,
        identity,
    )

    def hop(k, before):
        at = peers - 1 - k if reverse else k
        reached = at > here if reverse else at < here
        new = combine(
            before, jax.tree.map(lambda part, own: part[at].astype(own.dtype), everything, shard)
        )
        return jax.tree.map(lambda a, b: jnp.where(reached, a, b), new, before)

    return lax.fori_loop(0, peers, hop, start)


def centred_conv(padded, weights, series_count):
    summed = jnp.zeros((series_count, padded.shape[1]), jnp.float32)
    for offset in range(weights.shape[0]):
        summed = summed + weights[offset].astype(jnp.float32) * padded[
            offset : offset + series_count
        ].astype(jnp.float32)
    return jax.nn.silu(summed)


def local_sweep(inputs, entry_state, readout_state, log_fade_factor, softplus_increment):
    seq_len = inputs.shape[0]
    blocks = seq_len // BLOCK
    heads_here = log_fade_factor.shape[0]
    groups_here = entry_state.shape[1] // STATE
    per_group = heads_here // groups_here
    values = inputs.reshape(blocks, BLOCK, groups_here, per_group, HEAD_DIM)
    b_blocks = entry_state.reshape(blocks, BLOCK, groups_here, STATE)
    c_blocks = readout_state.reshape(blocks, BLOCK, groups_here, STATE)
    decay_blocks = log_fade_factor.reshape(groups_here, per_group, blocks, BLOCK)
    step_blocks = softplus_increment.reshape(groups_here, per_group, blocks, BLOCK)
    cumulative = jnp.cumsum(decay_blocks, axis=-1)
    group_inner = jnp.einsum("bign,bjgn->gbij", c_blocks, b_blocks, precision=HIGHEST_MODE)
    spread = cumulative[..., :, None] - cumulative[..., None, :]
    lower_tri = jnp.arange(BLOCK)[:, None] >= jnp.arange(BLOCK)[None, :]
    mixing = (
        jnp.exp(jnp.where(lower_tri, spread, -jnp.inf))
        * step_blocks[..., None, :]
        * group_inner[:, None]
    )
    within = jnp.einsum("gkbij,bjgkp->bigkp", mixing, values, precision=HIGHEST_MODE)
    to_end = jnp.exp(cumulative[..., -1:] - cumulative) * step_blocks
    block_states = jnp.einsum(
        "gkbj,bjgkp,bjgn->bgkpn", to_end, values, b_blocks, precision=HIGHEST_MODE
    )
    block_decay = cumulative[..., -1]

    def advance(carried, pieces):
        state_piece, decay_piece = pieces
        return (carried * jnp.exp(decay_piece)[..., None, None] + state_piece, carried)

    zero_state = jnp.zeros((groups_here, per_group, HEAD_DIM, STATE), jnp.float32)
    final_state, entering = lax.scan(
        advance, zero_state, (block_states, jnp.moveaxis(block_decay, -1, 0))
    )
    before = jnp.cumsum(block_decay, axis=-1) - block_decay
    return (
        (within, entering, cumulative, before, c_blocks),
        (jnp.sum(block_decay, axis=-1), final_state),
    )


def finish_sweep(parts, carried):
    within, entering, cumulative, before, c_blocks = parts
    entering = entering + carried[None] * jnp.exp(jnp.moveaxis(before, -1, 0))[..., None, None]
    readout = jnp.einsum("bign,bgkpn->bigkp", c_blocks, entering, precision=HIGHEST_MODE)
    readout = readout * jnp.exp(jnp.transpose(cumulative, (2, 3, 0, 1)))[..., None]
    combined = within + readout
    return combined.reshape(combined.shape[0] * combined.shape[1], -1)


def blend_parts_list(
    channel_feed_bordered,
    write_coefficient_bordered,
    emission_coefficient_bordered,
    channel_feed_taps,
    write_coefficient_taps,
    emission_coefficient_taps,
    raw_increments,
    channel_log_fade_speed,
    extra_log_fade,
    series_count,
):
    inputs = centred_conv(channel_feed_bordered, channel_feed_taps, series_count)
    entry_state = centred_conv(write_coefficient_bordered, write_coefficient_taps, series_count)
    readout_state = centred_conv(
        emission_coefficient_bordered, emission_coefficient_taps, series_count
    )
    softplus_increment = jax.nn.softplus(raw_increments.astype(jnp.float32))
    log_fade_factor = (
        -softplus_increment * jnp.exp(channel_log_fade_speed)[..., None] + extra_log_fade
    )
    onward_pass = local_sweep(
        inputs, entry_state, readout_state, log_fade_factor[0], softplus_increment[0]
    )
    backward_pass = local_sweep(
        jnp.flip(inputs, 0),
        jnp.flip(entry_state, 0),
        jnp.flip(readout_state, 0),
        jnp.flip(log_fade_factor[1], -1),
        jnp.flip(softplus_increment[1], -1),
    )
    return (onward_pass, backward_pass)


def gated_norm(mixed_sum, result_switch_mapped, cluster_scaling_factor):
    gated = mixed_sum * jax.nn.silu(result_switch_mapped.astype(jnp.float32))
    grouped = gated.reshape(gated.shape[0], -1, INNER // GROUPS)
    normalized = grouped * lax.rsqrt(jnp.mean(grouped * grouped, axis=-1, keepdims=True) + EPSILON)
    return (normalized.reshape(gated.shape) * cluster_scaling_factor).astype(jnp.bfloat16)


def rms_scale(stream, gain):
    values = stream.astype(jnp.float32)
    return (
        values * lax.rsqrt(jnp.mean(values * values, axis=-1, keepdims=True) + EPSILON) * gain
    ).astype(jnp.bfloat16)


def link_states(former, latter):
    former_total, former_state = former
    latter_total, latter_state = latter
    return (
        former_total + latter_total,
        former_state * jnp.exp(latter_total)[..., None, None] + latter_state,
    )


def per_device(
    skip_stream_entry,
    result_switch_mapped,
    channel_feed_mapped,
    write_coefficient_mapped,
    emission_coefficient_mapped,
    channel_feed_taps,
    write_coefficient_taps,
    emission_coefficient_taps,
    raw_increments,
    channel_log_fade_speed,
    extra_log_fade,
    cluster_scaling_factor,
    blend_result_matrix,
    routing_scaling_factor,
    specialist_switch_matrix,
    specialist_widen_matrix,
    specialist_contract_matrix,
    picked_specialists,
    router_affinities,
):
    series_count = channel_feed_mapped.shape[0]
    rim_width = CONV_W // 2
    sources = (channel_feed_mapped, write_coefficient_mapped, emission_coefficient_mapped)
    edges = jnp.concatenate(
        [jnp.concatenate([source[:rim_width], source[-rim_width:]], 0) for source in sources], 1
    )
    rimmed = with_halo(edges, (("sp", 0),), rim_width)
    padded_list = []
    column_start = 0
    for source in sources:
        width_here = source.shape[1]
        upper_rim = rimmed[:rim_width, column_start : column_start + width_here]
        lower_rim = rimmed[-rim_width:, column_start : column_start + width_here]
        padded_list.append(jnp.concatenate([upper_rim, source, lower_rim], 0))
        column_start = column_start + width_here
    onward_pass, backward_pass = blend_parts_list(
        padded_list[0],
        padded_list[1],
        padded_list[2],
        channel_feed_taps,
        write_coefficient_taps,
        emission_coefficient_taps,
        raw_increments,
        channel_log_fade_speed,
        extra_log_fade,
        series_count,
    )
    fwd_total, fwd_final = onward_pass[1]
    bwd_total, bwd_final = backward_pass[1]
    identity_pair = (jnp.zeros_like(fwd_total), jnp.zeros_like(fwd_final))
    carried_fwd = prefix((fwd_total, fwd_final), "sp", link_states, identity_pair, False)[1]
    carried_bwd = prefix((bwd_total, bwd_final), "sp", link_states, identity_pair, True)[1]
    mixed_sum = finish_sweep(onward_pass[0], carried_fwd) + jnp.flip(
        finish_sweep(backward_pass[0], carried_bwd), 0
    )
    mixed_rows = gated_norm(mixed_sum, result_switch_mapped, cluster_scaling_factor)
    rows_here = skip_stream_entry.shape[0]
    projected = lax.psum_scatter(
        jnp.dot(mixed_rows, blend_result_matrix, preferred_element_type=jnp.float32).astype(
            jnp.bfloat16
        ),
        "tp",
        scatter_dimension=0,
        tiled=True,
    ).astype(jnp.float32)
    after_mixer = (skip_stream_entry.astype(jnp.float32) + projected).astype(jnp.bfloat16)
    normed = rms_scale(after_mixer, routing_scaling_factor)
    experts_here = specialist_switch_matrix.shape[0]
    expert_count = experts_here * lax.axis_size("sp")
    capacity = max(2, 3 * TOP * rows_here // (2 * expert_count))
    slot_total = capacity * expert_count
    flat_routes = picked_specialists.reshape(-1)
    one_hot = (flat_routes[:, None] == jnp.arange(expert_count, dtype=jnp.int32)[None, :]).astype(
        jnp.int32
    )
    earlier_count = jnp.cumsum(one_hot, axis=0) - one_hot
    slot_rank = jnp.sum(earlier_count * one_hot, axis=1)
    position = slot_rank * expert_count + flat_routes
    slot_match = (position[:, None] == jnp.arange(slot_total, dtype=jnp.int32)[None, :]).astype(
        jnp.bfloat16
    )
    buffer = jnp.einsum(
        "rks,rd->sd",
        slot_match.reshape(rows_here, TOP, slot_total),
        normed,
        preferred_element_type=jnp.float32,
    ).astype(jnp.bfloat16)
    buffer = buffer.reshape(capacity, expert_count, WIDTH)
    received = lax.all_to_all(buffer, "sp", split_axis=1, concat_axis=0, tiled=True)
    data_block = lax.all_gather(received, "tp", axis=0, tiled=True)
    gate_part = jnp.einsum(
        "red,edf->ref", data_block, specialist_switch_matrix, preferred_element_type=jnp.float32
    )
    up_part = jnp.einsum(
        "red,edf->ref", data_block, specialist_widen_matrix, preferred_element_type=jnp.float32
    )
    hidden = (jax.nn.silu(gate_part) * up_part).astype(jnp.bfloat16)
    expert_out = lax.psum_scatter(
        jnp.einsum(
            "ref,efd->red", hidden, specialist_contract_matrix, preferred_element_type=jnp.float32
        ).astype(jnp.bfloat16),
        "tp",
        scatter_dimension=0,
        tiled=True,
    )
    returned = lax.all_to_all(expert_out, "sp", split_axis=0, concat_axis=1, tiled=True)
    picked = jnp.dot(
        slot_match, returned.reshape(slot_total, WIDTH), preferred_element_type=jnp.float32
    )
    weights = router_affinities / jnp.sum(router_affinities, axis=-1, keepdims=True)
    mixture = jnp.sum(weights[..., None] * picked.reshape(rows_here, TOP, WIDTH), axis=1)
    return (after_mixer.astype(jnp.float32) + mixture).astype(jnp.bfloat16)


def solution(mesh):
    in_specs = (
        P(("sp", "tp"), None),
        P("sp", "tp"),
        P("sp", "tp"),
        P("sp", "tp"),
        P("sp", "tp"),
        P(None, "tp"),
        P(None, "tp"),
        P(None, "tp"),
        P(None, "tp", "sp"),
        P(None, "tp"),
        P(None, "tp", "sp"),
        P("tp"),
        P("tp", None),
        P(),
        P("sp", None, "tp"),
        P("sp", None, "tp"),
        P("sp", "tp", None),
        P(("sp", "tp"), None),
        P(("sp", "tp"), None),
    )
    out_specs = P(("sp", "tp"), None)
    return jax.shard_map(
        per_device, mesh=mesh, in_specs=in_specs, out_specs=out_specs, check_vma=False
    )
```

profile of v0, /device:TPU:0, one launch (start us, length us, event | category | flops | bytes accessed | tf_op | source)
XLA Modules:
  0.0 437.1 jit_solution(5094532863845228223)
XLA Ops:
  9.1 5.6 %collective-permute-start = (bf16[2,1024]{0,1:T(8,128)(2,1)}, bf16[2,1024]{0,1:T(8,128)(2,1)}, u32[]{:S(2)}, u32[]{:S(2)}) collective-permute-start(bf16[2,1024]{0,1:T(8,128)(2,1)} %copy.175), channel_id=1, source_target_pairs={{0,8},{8,16},{16,24},{1,9},{9,17},{17,25},{2,10},{10,18},{18,26},{... | collective-permute-start | bytes 12296 | tf_op jit(solution)/shard_map/ppermute | solution.py:25
  15.5 1.3 collective-permute-start.1
  16.8 1.5 slice_convert_fusion.14
  18.3 1.5 slice_convert_fusion.9
  19.8 1.5 slice_convert_fusion.4
  22.8 2.4 reduce_window_sum.45
  27.1 2.4 reduce_window_sum.47
  30.8 9.6 %all-gather.4 = bf16[4,2,4]{2,1,0:T(2,128)(2,1)} all-gather(bf16[1,2,4]{2,1,0:T(2,128)(2,1)S(1)} %bitcast.210), channel_id=2, replica_groups=mesh['sp'=4,'tp'=8] {'sp'}, dimensions={0}, use_global_device_ids=true | all-gather | bytes 80 | tf_op jit(solution)/shard_map/all_gather | solution.py:36
  40.5 8.3 %all-gather.5 = bf16[4,2,4]{2,1,0:T(2,128)(2,1)} all-gather(bf16[1,2,4]{2,1,0:T(2,128)(2,1)S(1)} %bitcast.211), channel_id=4, replica_groups=mesh['sp'=4,'tp'=8] {'sp'}, dimensions={0}, use_global_device_ids=true | all-gather | bytes 80 | tf_op jit(solution)/shard_map/all_gather | solution.py:36
  48.8 2.1 copy.176
  56.0 2.0 copy.210
  59.6 1.5 fusion.101
  61.1 1.5 copy.184
  62.6 2.0 divide_multiply_fusion.2
  64.6 2.1 reshape.175
  66.7 4.7 %rev.24 = f32[512,256]{1,0:T(8,128)} reverse(f32[512,256]{1,0:T(8,128)} %divide_multiply_fusion.2), dimensions={0} | reverse | bytes 1048576 | tf_op jit(solution)/shard_map/jit(_flip)/rev | solution.py:144
  71.7 3.1 divide_multiply_fusion.1
  74.7 2.1 reshape.176
  76.8 4.7 %rev.25 = f32[512,256]{1,0:T(8,128)} reverse(f32[512,256]{1,0:T(8,128)} %divide_multiply_fusion.1), dimensions={0} | reverse | bytes 1048576 | tf_op jit(solution)/shard_map/jit(_flip)/rev | solution.py:143
  83.4 4.7 %divide_multiply_fusion = f32[512,512]{0,1:T(8,128)} fusion(bf16[512,512]{0,1:T(8,128)(2,1)} %copy.176, bf16[2,512]{0,1:T(8,128)(2,1)S(1)} %slice.207, bf16[2,512]{0,1:T(8,128)(2,1)S(1)} %slice.203, f32[512]{0:T(512)S(1)} %bitcast.198, f32[512]{0:T(512)S(1)} %bitcast.199, f32[512]{0:T(512)S(1)} %bitcast.196, f32[512]{0:T(512)S(1)} %bitcast.197, ...), kind=kLoop, calls=%fused_computation.78 | loop fusion | flops 7864320 | bytes 1587200 | tf_op jit(solution)/shard_map/jit(silu)/mul | solution.py:63
  88.1 2.6 reshape.174
  90.7 9.4 %rev.21 = f32[512,512]{0,1:T(8,128)} reverse(f32[512,512]{0,1:T(8,128)} %divide_multiply_fusion), dimensions={0} | reverse | bytes 2097152 | tf_op jit(solution)/shard_map/jit(_flip)/rev | solution.py:142
  100.1 3.3 fusion.72
  103.4 1.4 broadcast_multiply_fusion.1
  104.8 2.1 fusion.40
  106.9 1.1 broadcast.90.clone.1
  108.0 9.8 %while.56 = (s32[]{:T(128)}, f32[2,4,64,128]{3,2,1,0:T(8,128)S(1)}, f32[4,2,4,64,128]{4,3,2,1,0:T(8,128)}, f32[4,2,4]{2,1,0:T(2,128)}, f32[4,2,4,64,128]{4,3,2,1,0:T(8,128)}, /*index=5*/s32[]{:T(128)}, s32[]{:T(128)}) while((s32[]{:T(128)}, f32[2,4,64,128]{3,2,1,0:T(8,128)S(1)}, f32[4,2,4,64,128]{4,3,2,1,0:T(8,128)}, ...), condition=%wide.region_2.3_spmd.clone, body=%wide.region_1.2_spmd.clone.sunk | while | flops 262147 | bytes 1311424 | solution.py:98
  109.4 1.0 bitcast_add_fusion.5
  111.9 1.0 bitcast_add_fusion.5
  114.3 1.0 bitcast_add_fusion.5
  116.7 1.0 bitcast_add_fusion.5
  117.8 10.1 %all-gather.1 = bf16[8,4,64,128]{3,2,1,0:T(8,128)(2,1)} all-gather(bf16[2,4,64,128]{3,2,1,0:T(8,128)(2,1)S(1)} %convert_element_type.229), channel_id=3, replica_groups=mesh['sp'=4,'tp'=8] {'sp'}, dimensions={0}, use_global_device_ids=true | all-gather | bytes 655360 | tf_op jit(solution)/shard_map/all_gather | solution.py:36
  127.9 6.8 %while.57 = (s32[]{:T(128)}, f32[2,4,64,128]{3,2,1,0:T(8,128)S(1)}, s32[]{:T(128)}, bf16[4,2,4]{2,1,0:T(2,128)(2,1)}, bf16[4,2,4,64,128]{4,3,2,1,0:T(8,128)(2,1)}, /*index=5*/s32[]{:T(128)}, s32[]{:T(128)}) while((s32[]{:T(128)}, f32[2,4,64,128]{3,2,1,0:T(8,128)S(1)}, s32[]{:T(128)}, bf16[4,2,4]{2,1,0:T(2,128)(2,1)}, ...), condition=%wide.region_5.6_spmd.clone, body=%wide.region_4.5_spmd.clone.sunk | while | flops 327692 | bytes 655545 | solution.py:54
  134.8 5.6 %fusion.20 = f32[4,128,2,4,64]{1,4,3,2,0:T(8,128)S(1)} fusion(f32[4,128,2,4,64]{1,0,4,3,2:T(4,128)} %reshape.174, f32[2,4,128,128]{3,2,0,1:T(8,128)} %fusion.72, f32[2,4,4,128]{3,1,0,2:T(4,128)S(1)} %bitcast.194, f32[2,4,4,128]{3,1,0,2:T(4,128)S(1)} %copy-done.21, pred[128,128]{1,0:T(8,128)(4,1)S(1)} %copy-done.19), kind=kOutput, calls=%fused_computation.37 | convolution fusion | flops 404750336 | bytes 2670592 | tf_op jit(solution)/shard_map/gkbij,bjgkp->bigkp/dot_general | solution.py:86
  140.5 1.3 fusion.29
  141.7 1.7 copy.196
  143.4 1.3 reshape.180
  144.7 2.1 reshape.181
  146.9 2.5 reshape.178
  149.4 3.1 fusion.69
  152.5 1.4 broadcast_multiply_fusion
  153.9 2.1 fusion.37
  156.0 1.1 broadcast.90.clone
  157.1 9.8 %while.58 = (s32[]{:T(128)}, f32[2,4,64,128]{3,2,1,0:T(8,128)S(1)}, f32[4,2,4,64,128]{4,3,2,1,0:T(8,128)}, f32[4,2,4]{2,1,0:T(2,128)}, f32[4,2,4,64,128]{4,3,2,1,0:T(8,128)}, /*index=5*/s32[]{:T(128)}, s32[]{:T(128)}) while((s32[]{:T(128)}, f32[2,4,64,128]{3,2,1,0:T(8,128)S(1)}, f32[4,2,4,64,128]{4,3,2,1,0:T(8,128)}, ...), condition=%wide.region_9.10_spmd.clone, body=%wide.region_8.9_spmd.clone.sunk | while | flops 262147 | bytes 1311424 | solution.py:98
  166.9 10.7 %all-gather.3 = bf16[8,4,64,128]{3,2,1,0:T(8,128)(2,1)} all-gather(bf16[2,4,64,128]{3,2,1,0:T(8,128)(2,1)S(1)} %convert_element_type.232), channel_id=5, replica_groups=mesh['sp'=4,'tp'=8] {'sp'}, dimensions={0}, use_global_device_ids=true | all-gather | bytes 655360 | tf_op jit(solution)/shard_map/all_gather | solution.py:36
  177.6 6.8 %while.59 = (s32[]{:T(128)}, f32[2,4,64,128]{3,2,1,0:T(8,128)S(1)}, s32[]{:T(128)}, bf16[4,2,4]{2,1,0:T(2,128)(2,1)}, bf16[4,2,4,64,128]{4,3,2,1,0:T(8,128)(2,1)...) while((s32[]{:T(128)}, f32[2,4,64,128]{3,2,1,0:T(8,128)S(1)}, s32[]{:T(128)}, ...), condition=%wide.region_12.13_spmd.clone, body=%wide.region_11.12_spmd.clone.sunk | while | flops 327696 | bytes 655607 | solution.py:54
  184.4 5.6 %fusion.23 = f32[4,128,2,4,64]{1,4,3,2,0:T(8,128)S(1)} fusion(f32[4,128,2,4,64]{1,0,4,3,2:T(4,128)} %reshape.178, f32[2,4,128,128]{3,2,0,1:T(8,128)} %fusion.69, f32[2,4,4,128]{3,1,0,2:T(4,128)S(1)} %bitcast.193, f32[2,4,4,128]{3,1,0,2:T(4,128)S(1)} %copy-done.20, pred[128,128]{1,0:T(8,128)(4,1)S(1)} %copy-done.19), kind=kOutput, calls=%fused_computation.38 | convolution fusion | flops 404750336 | bytes 2670592 | tf_op jit(solution)/shard_map/gkbij,bjgkp->bigkp/dot_general | solution.py:86
  190.1 1.3 fusion.27
  192.1 6.0 %rev.26 = f32[512,512]{0,1:T(8,128)} reverse(f32[512,512]{0,1:T(8,128)S(1)} %bitcast.183), dimensions={0} | reverse | bytes 2097152 | tf_op jit(solution)/shard_map/jit(_flip)/rev | solution.py:227
  198.1 2.1 bitcast_reduce_fusion
  200.5 2.6 convolution_convert_fusion
  204.2 35.4 %reduce-scatter.3.cloned.1.call-done = bf16[64,2048]{1,0:T(8,128)(2,1)} async-done(((bf16[512,2048]{1,0:T(8,128)(2,1)}), bf16[64,2048]{1,0:T(8,128)(2,1)}) %reduce-scatter.3.cloned.1.call-update) | async-done | bytes 262160 | tf_op jit(solution)/shard_map/reduce_scatter | solution.py:232
  239.6 1.1 fusion.61
  240.7 1.4 fusion.6
  242.6 12.0 %all_to_all.33 = bf16[24,8,2048]{2,0,1:T(8,128)(2,1)S(1)} all-to-all(bf16[24,8,2048]{2,0,1:T(8,128)(2,1)S(1)} %copy.213), channel_id=1, replica_groups=mesh['sp'=4,'tp'=8] {'sp'}, dimensions={1} | all-to-all | bytes 1572864 | tf_op jit(solution)/shard_map/all_to_all | solution.py:263
  255.9 63.8 %all-gather.8.cloned.1.call-done = bf16[768,2,2048]{2,0,1:T(8,128)(2,1)} async-done(((bf16[96,2,2048]{2,0,1:T(8,128)(2,1)}), bf16[768,2,2048]{2,0,1:T(8,128)(2,1)}) %all-gather.8.cloned.1.call-update) | async-done | bytes 6291472 | tf_op jit(solution)/shard_map/all_gather | solution.py:264
  319.7 9.1 %fusion.107 = f32[2,768,512]{2,1,0:T(8,128)} fusion(bf16[768,2,2048]{2,0,1:T(8,128)(2,1)} %all-gather.8.cloned.1.call-done, bf16[2,2048,512]{2,1,0:T(8,128)(2,1)} %param.42), kind=kOutput, calls=%fused_computation.197 | convolution fusion | flops 3221225472 | bytes 13631488 | tf_op jit(solution)/shard_map/red,edf->ref/dot_general | solution.py:268
  328.7 12.5 %convert_bitcast_fusion = bf16[768,2,2048]{2,0,1:T(8,128)(2,1)} fusion(bf16[2,512,2048]{2,1,0:T(8,128)(2,1)} %param.43, f32[2,768,512]{2,1,0:T(8,128)} %fusion.107, bf16[768,2,2048]{2,0,1:T(8,128)(2,1)} %all-gather.8.cloned.1.call-done, bf16[2,2048,512]{2,1,0:T(8,128)(2,1)} %param.41), kind=kOutput, calls=%fused_computation.12 | convolution fusion | flops 6450315264 | bytes 24117248 | tf_op jit(solution)/shard_map/ref,efd->red/dot_general | solution.py:273
  341.2 68.5 %reduce-scatter.5.cloned.1.call-done = bf16[96,2,2048]{2,0,1:T(8,128)(2,1)} async-done(((bf16[768,2,2048]{2,0,1:T(8,128)(2,1)}), bf16[96,2,2048]{2,0,1:T(8,128)(2,1)}) %reduce-scatter.5.cloned.1.call-update) | async-done | bytes 786448 | tf_op jit(solution)/shard_map/reduce_scatter | solution.py:272
  409.8 2.8 copy.215
  412.6 3.8 all-to-all-start.1
  416.4 9.1 %all-to-all-done.1 = bf16[96,2,2048]{2,1,0:T(2,128)(2,1)S(1)} async-done(((bf16[96,2,2048]{2,1,0:T(2,128)(2,1)}), bf16[96,2,2048]{2,1,0:T(2,128)(2,1)S(1)}, u32[]{:S(2)}, u32[]{:S(2)}) %all-to-all-start.1) | async-done | bytes 786464 | tf_op jit(solution)/shard_map/all_to_all | solution.py:280
  425.5 1.7 copy.260
  427.2 2.3 reshape.218
  (171 shorter events, 50.4 us)
Async XLA Ops:
  6.5 193.9 %copy-start = (bf16[512,2048]{1,0:T(8,128)(2,1)S(1)}, bf16[512,2048]{1,0:T(8,128)(2,1)}, u32[]{:S(2)}) copy-start(bf16[512,2048]{1,0:T(8,128)(2,1)} %param.39) | copy-start | bytes 6291460
  6.5 56.1 %copy-start.9 = (bf16[512,256]{1,0:T(8,128)(2,1)S(1)}, bf16[512,256]{1,0:T(8,128)(2,1)}, u32[]{:S(2)}) copy-start(bf16[512,256]{1,0:T(8,128)(2,1)} %param.31) | copy-start | bytes 786436
  6.5 233.0 %reduce-scatter.3.cloned.1.call-start = ((), (), s32[]{:S(2)}) async-start(), calls=%async_computation.4 | async-start | bytes 2359296 | tf_op jit(solution)/shard_map/reduce_scatter | solution.py:232
  9.1 49.0 %collective-permute-start = (bf16[2,1024]{0,1:T(8,128)(2,1)}, bf16[2,1024]{0,1:T(8,128)(2,1)}, u32[]{:S(2)}, u32[]{:S(2)}) collective-permute-start(bf16[2,1024]{0,1:T(8,128)(2,1)} %copy.175), channel_id=1, source_target_pairs={{0,8},{8,16},{16,24},{1,9},{9,17},{17,25},{2,10},{10,18},{18,26},{... | collective-permute-start | bytes 12296 | tf_op jit(solution)/shard_map/ppermute | solution.py:25
  15.5 44.0 %collective-permute-start.1 = (bf16[2,1024]{0,1:T(8,128)(2,1)}, bf16[2,1024]{0,1:T(8,128)(2,1)}, u32[]{:S(2)}, u32[]{:S(2)}) collective-permute-start(bf16[2,1024]{0,1:T(8,128)(2,1)} %copy.178), channel_id=1, source_target_pairs={{8,0},{16,8},{24,16},{9,1},{17,9},{25,17},{10,2},{18,10},{26,18},{... | collective-permute-start | bytes 12296 | tf_op jit(solution)/shard_map/ppermute | solution.py:28
  22.8 3.7 copy-start.15
  27.1 2.6 copy-start.13
  64.5 18.8 %copy-start.23 = (f32[1,512]{1,0:T(1,128)S(1)}, f32[1,512]{1,0:T(1,128)}, u32[]{:S(2)}) copy-start(f32[1,512]{1,0:T(1,128)} %get-tuple-element.481) | copy-start | bytes 6148
  64.5 18.9 %copy-start.24 = (f32[1,512]{1,0:T(1,128)S(1)}, f32[1,512]{1,0:T(1,128)}, u32[]{:S(2)}) copy-start(f32[1,512]{1,0:T(1,128)} %get-tuple-element.482) | copy-start | bytes 6148
  64.6 18.9 %copy-start.25 = (f32[1,512]{1,0:T(1,128)S(1)}, f32[1,512]{1,0:T(1,128)}, u32[]{:S(2)}) copy-start(f32[1,512]{1,0:T(1,128)} %get-tuple-element.483) | copy-start | bytes 6148
  64.6 18.9 %copy-start.26 = (f32[1,512]{1,0:T(1,128)S(1)}, f32[1,512]{1,0:T(1,128)}, u32[]{:S(2)}) copy-start(f32[1,512]{1,0:T(1,128)} %get-tuple-element.484) | copy-start | bytes 6148
  64.6 18.9 %copy-start.27 = (f32[1,512]{1,0:T(1,128)S(1)}, f32[1,512]{1,0:T(1,128)}, u32[]{:S(2)}) copy-start(f32[1,512]{1,0:T(1,128)} %get-tuple-element.485) | copy-start | bytes 6148
  88.1 15.3 %copy-start.10 = (f32[4,128,2,4]{1,0,3,2:T(4,128)S(1)}, f32[4,128,2,4]{1,0,3,2:T(4,128)}, u32[]{:S(2)}) copy-start(f32[4,128,2,4]{1,0,3,2:T(4,128)} %get-tuple-element.476) | copy-start | bytes 49156
  100.1 4.7 %copy-start.3 = (f32[4,128,2,128]{3,2,1,0:T(2,128)S(1)}, f32[4,128,2,128]{3,2,1,0:T(2,128)}, u32[]{:S(2)}) copy-start(f32[4,128,2,128]{3,2,1,0:T(2,128)} %reshape.176) | copy-start | bytes 1572868
  117.8 17.0 %copy-start.16 = (f32[1,8,512]{2,1,0:T(8,128)S(1)}, f32[1,8,512]{2,1,0:T(8,128)}, u32[]{:S(2)}) copy-start(f32[1,8,512]{2,1,0:T(8,128)} %copy-done.15) | copy-start | bytes 49156
  117.8 17.0 %copy-start.19 = (pred[128,128]{1,0:T(8,128)(4,1)S(1)}, pred[128,128]{1,0:T(8,128)(4,1)}, u32[]{:S(2)}) copy-start(pred[128,128]{1,0:T(8,128)(4,1)} %iota_compare_fusion.3) | copy-start | bytes 49156
  117.8 17.0 %copy-start.21 = (f32[2,4,4,128]{3,1,0,2:T(4,128)S(1)}, f32[2,4,4,128]{3,1,0,2:T(4,128)}, u32[]{:S(2)}) copy-start(f32[2,4,4,128]{3,1,0,2:T(4,128)} %copy.180) | copy-start | bytes 49156
  127.9 12.5 %copy-start.2 = (f32[4,128,2,128]{3,2,1,0:T(2,128)S(1)}, f32[4,128,2,128]{3,2,1,0:T(2,128)}, u32[]{:S(2)}) copy-start(f32[4,128,2,128]{3,2,1,0:T(2,128)} %reshape.175) | copy-start | bytes 1572868
  127.9 12.5 %copy-start.12 = (f32[4,128,2,4]{1,3,2,0:T(4,128)S(1)}, f32[4,128,2,4]{1,3,2,0:T(4,128)}, u32[]{:S(2)}) copy-start(f32[4,128,2,4]{1,3,2,0:T(4,128)} %copy.195) | copy-start | bytes 49156
  127.9 12.5 %copy-start.18 = (f32[4,2,4]{2,1,0:T(2,128)S(1)}, f32[4,2,4]{2,1,0:T(2,128)}, u32[]{:S(2)}) copy-start(f32[4,2,4]{2,1,0:T(2,128)} %copy.193) | copy-start | bytes 388
  134.7 5.7 %copy-start.5 = (f32[4,2,4,64,128]{4,3,2,1,0:T(8,128)S(1)}, f32[4,2,4,64,128]{4,3,2,1,0:T(8,128)}, u32[]{:S(2)}) copy-start(f32[4,2,4,64,128]{4,3,2,1,0:T(8,128)} %get-tuple-element.287) | copy-start | bytes 3145732
  149.4 4.5 %copy-start.4 = (f32[4,128,2,128]{3,2,1,0:T(2,128)S(1)}, f32[4,128,2,128]{3,2,1,0:T(2,128)}, u32[]{:S(2)}) copy-start(f32[4,128,2,128]{3,2,1,0:T(2,128)} %reshape.181) | copy-start | bytes 1572868
  166.9 17.5 %copy-start.14 = (f32[8,512]{1,0:T(8,128)S(1)}, f32[8,512]{1,0:T(8,128)}, u32[]{:S(2)}) copy-start(f32[8,512]{1,0:T(8,128)} %copy-done.13) | copy-start | bytes 49156
  166.9 17.5 %copy-start.20 = (f32[2,4,4,128]{3,1,0,2:T(4,128)S(1)}, f32[2,4,4,128]{3,1,0,2:T(4,128)}, u32[]{:S(2)}) copy-start(f32[2,4,4,128]{3,1,0,2:T(4,128)} %copy.197) | copy-start | bytes 49156
  177.6 12.5 %copy-start.11 = (f32[4,128,2,4]{1,3,2,0:T(4,128)S(1)}, f32[4,128,2,4]{1,3,2,0:T(4,128)}, u32[]{:S(2)}) copy-start(f32[4,128,2,4]{1,3,2,0:T(4,128)} %copy.208) | copy-start | bytes 49156
  177.6 12.5 %copy-start.17 = (f32[4,2,4]{2,1,0:T(2,128)S(1)}, f32[4,2,4]{2,1,0:T(2,128)}, u32[]{:S(2)}) copy-start(f32[4,2,4]{2,1,0:T(2,128)} %copy.206) | copy-start | bytes 388
  184.4 5.7 %copy-start.6 = (f32[4,2,4,64,128]{4,3,2,1,0:T(8,128)S(1)}, f32[4,2,4,64,128]{4,3,2,1,0:T(8,128)}, u32[]{:S(2)}) copy-start(f32[4,2,4,64,128]{4,3,2,1,0:T(8,128)} %get-tuple-element.290) | copy-start | bytes 3145732
  192.1 8.1 %copy-start.30 = (f32[512]{0:T(512)S(1)}, f32[512]{0:T(512)}, u32[]{:S(2)}) copy-start(f32[512]{0:T(512)} %param.38) | copy-start | bytes 6148
  200.4 2.7 copy-start.28
  200.5 39.1 %copy-start.7 = (bf16[64,2048]{1,0:T(8,128)(2,1)S(1)}, bf16[64,2048]{1,0:T(8,128)(2,1)}, u32[]{:S(2)}) copy-start(bf16[64,2048]{1,0:T(8,128)(2,1)} %param.27) | copy-start | bytes 786436
  200.5 40.3 %copy-start.22 = (f32[2048]{0:T(1024)S(1)}, f32[2048]{0:T(1024)}, u32[]{:S(2)}) copy-start(f32[2048]{0:T(1024)} %param.40) | copy-start | bytes 24580
  203.1 116.5 %all-gather.8.cloned.1.call-start = ((), (), s32[]{:S(2)}) async-start(), calls=%async_computation.5 | async-start | bytes 7077888 | tf_op jit(solution)/shard_map/all_gather | solution.py:264
  255.6 154.2 %reduce-scatter.5.cloned.1.call-start = ((), (), s32[]{:S(2)}) async-start(), calls=%async_computation.6 | async-start | bytes 7077888 | tf_op jit(solution)/shard_map/reduce_scatter | solution.py:272
  341.2 75.2 %copy-start.29 = (f32[64,2]{0,1:T(2,128)S(1)}, f32[64,2]{0,1:T(2,128)}, u32[]{:S(2)}) copy-start(f32[64,2]{0,1:T(2,128)} %param.45) | copy-start | bytes 1540
  412.6 17.2 %copy-start.8 = (bf16[64,2048]{1,0:T(8,128)(2,1)S(1)}, bf16[64,2048]{1,0:T(8,128)(2,1)}, u32[]{:S(2)}) copy-start(bf16[64,2048]{1,0:T(8,128)(2,1)} %reduce-scatter.3.cloned.1.call-done) | copy-start | bytes 786436
  412.6 12.9 %all-to-all-start.1 = ((bf16[96,2,2048]{2,1,0:T(2,128)(2,1)}), bf16[96,2,2048]{2,1,0:T(2,128)(2,1)S(1)}, u32[]{:S(2)}, u32[]{:S(2)}) async-start(bf16[96,2,2048]{2,1,0:T(2,128)(2,1)} %copy.215), calls=%async_computation.3 | async-start | bytes 1572864 | tf_op jit(solution)/shard_map/all_to_all | solution.py:280
  416.4 14.2 %copy-start.1 = (bf16[512,2048]{1,0:T(8,128)(2,1)S(1)}, bf16[512,2048]{1,0:T(8,128)(2,1)}, u32[]{:S(2)}) copy-start(bf16[512,2048]{1,0:T(8,128)(2,1)} %param.39) | copy-start | bytes 6291460
Sparse Core Ops, SparseCore 0:
  203.2 36.2 reduce-scatter.2
  255.7 63.9 all-gather.7
  341.3 68.3 reduce-scatter.4
where the time goes:
time: 441 us; the launch traced here: 437 us
  waiting for transfers between devices  177 us (40%)
  local copies, waits for them, and re-layouts  76.9 us (17%)
  other arithmetic  57.6 us (13%)
  blocking collectives  50.7 us (11%)
  matrix products  50.2 us (11%)
  between operations  13.7 us (3%)
  starting transfers between devices  11 us (2%)
    reduce_scatter x1, waiting for transfers between devices, per_device(): lax.psum_scatter(jnp.einsum('ref,efd->red', hidden, specialist_contract_m...  68.5 us
    all_gather x1, waiting for transfers between devices, per_device(): data_block = lax.all_gather(received, 'tp', axis=0, tiled=True)  63.8 us
    all_gather x4, blocking collectives, prefix(): lax.all_gather(part.astype(kind), axis)  38.7 us
    reduce_scatter x1, waiting for transfers between devices, per_device(): lax.psum_scatter(jnp.dot(mixed_rows, blend_result_matrix, preferred_eleme...  35.4 us
    dot_general x1, matrix products, per_device(): jnp.einsum('ref,efd->red', hidden, specialist_contract_matrix, preferred_...  12.5 us
    all_to_all x1, blocking collectives, per_device(): lax.all_to_all(buffer, 'sp', split_axis=1, concat_axis=0, tiled=True)  12 us
    dot_general x2, matrix products, local_sweep(): jnp.einsum('gkbij,bjgkp->bigkp', mixing, values, precision=HIGHEST_MODE)  11.3 us
    mul x3, other arithmetic, centred_conv(): return jax.nn.silu(summed)  9.7 us
  transfers between devices with their start and end apart: 6, of which 4 were waited for; matrix products, arithmetic and copies ran while one was open for 6% of the time, Pallas kernels for 0%

commit v1 on v0

v1 whole, which is shorter than its diff:
```python
import functools

import jax
import jax.numpy as jnp
from jax import lax
from jax.experimental import pallas as pl
from jax.experimental.pallas import tpu as pltpu
from jax.sharding import PartitionSpec as P

WIDTH = 2048
HEAD_DIM = 64
GROUPS = 16
STATE = 128
CONV_W = 5
BLOCK = 128
TOP = 2
INNER = 4096


EPSILON = 1e-06
HIGHEST_MODE = lax.Precision.HIGHEST


MESH_IDS = pl.DeviceIdType.MESH


def neighbour_rows(rows, axis, step):
    count = lax.axis_size(axis)
    pairs = [(i, i + step) for i in range(count) if 0 <= i + step < count]
    return lax.ppermute(rows, axis, pairs)


def spread_heads(columns, per_group):
    rows = columns.shape[0]
    lane = lax.broadcasted_iota(jnp.int32, (rows, per_group * HEAD_DIM), 1) // HEAD_DIM
    out = jnp.broadcast_to(columns[:, 0:1], lane.shape)
    for head in range(1, per_group):
        out = jnp.where(lane == head, jnp.broadcast_to(columns[:, head : head + 1], lane.shape), out)
    return out


def silu(value):
    return value * jax.nn.sigmoid(value)


def fill_padded(scratch, source, low, high):
    count, rim = source.shape[0], low.shape[0]
    scratch[8 : 8 + count, :] = source[...].astype(jnp.float32)
    scratch[8 - rim : 8, :] = low[...].astype(jnp.float32)
    scratch[8 + count : 8 + count + rim, :] = high[...].astype(jnp.float32)


def conv_block(scratch, taps, block):
    rim = taps.shape[0] // 2
    total = None
    for offset in range(taps.shape[0]):
        start = 8 - rim + offset + block * BLOCK
        term = taps[offset : offset + 1, :].astype(jnp.float32) * scratch[start : start + BLOCK, :]
        total = term if total is None else total + term
    return silu(total)


def sweep_kernel(
    x_ref, b_ref, c_ref, x_low, x_high, b_low, b_high, c_low, c_high, x_taps, b_taps, c_taps,
    fade_ref, y_ref, c_out, state_ref, reach_ref, x_pad, b_pad, c_pad, entry_scr,
):
    count, width = x_ref.shape
    blocks = count // BLOCK
    per_group = width // HEAD_DIM
    rows = 2 * per_group
    fill_padded(x_pad, x_ref, x_low, x_high)
    fill_padded(b_pad, b_ref, b_low, b_high)
    fill_padded(c_pad, c_ref, c_low, c_high)
    i_at = lax.broadcasted_iota(jnp.int32, (BLOCK, BLOCK), 0)
    j_at = lax.broadcasted_iota(jnp.int32, (BLOCK, BLOCK), 1)
    up_to = (i_at <= j_at).astype(jnp.float32)
    from_on = (i_at >= j_at).astype(jnp.float32)
    row_at = lax.broadcasted_iota(jnp.int32, (rows, BLOCK), 0)
    col_at = lax.broadcasted_iota(jnp.int32, (1, rows), 1)
    half_lane = lax.broadcasted_iota(jnp.int32, (BLOCK, 2 * HEAD_DIM), 1) < HEAD_DIM
    totals, parts, columns_kept, mixed = [], [], [], []
    for block in range(blocks):
        at = slice(block * BLOCK, (block + 1) * BLOCK)
        fade = fade_ref[0, 0:rows, at]
        step = fade_ref[0, rows : 2 * rows, at]
        onward = jnp.dot(fade, up_to, precision=HIGHEST_MODE, preferred_element_type=jnp.float32)
        back = jnp.dot(fade, from_on, precision=HIGHEST_MODE, preferred_element_type=jnp.float32)
        cum = jnp.where(row_at < per_group, onward, back)
        stacked = jnp.concatenate(
            [cum, step, jnp.zeros((BLOCK - 2 * rows, BLOCK), jnp.float32)], axis=0
        )
        turned = jnp.transpose(stacked)
        cum_col, step_col = turned[:, 0:rows], turned[:, rows : 2 * rows]
        total = jnp.where(col_at < per_group, cum_col[BLOCK - 1 : BLOCK, :], cum_col[0:1, :])
        to_end = jnp.exp(total - cum_col) * step_col
        x = conv_block(x_pad, x_taps, block)
        b = conv_block(b_pad, b_taps, block)
        c = conv_block(c_pad, c_taps, block).astype(jnp.bfloat16)
        c_out[at, :] = c
        b_turned = jnp.transpose(b).astype(jnp.bfloat16)
        weighted = jnp.concatenate(
            [
                x * spread_heads(to_end[:, 0:per_group], per_group),
                x * spread_heads(to_end[:, per_group:rows], per_group),
            ],
            axis=1,
        ).astype(jnp.bfloat16)
        parts.append(jnp.dot(b_turned, weighted, preferred_element_type=jnp.float32))
        inner = jnp.dot(c, b_turned, preferred_element_type=jnp.float32)
        mixing = []
        for head in range(per_group):
            other = per_group + head
            gap = jnp.where(
                i_at >= j_at,
                cum_col[:, head : head + 1] - cum[head : head + 1, :],
                cum_col[:, other : other + 1] - cum[other : other + 1, :],
            )
            own, opposite = step[head : head + 1, :], step[other : other + 1, :]
            amount = jnp.where(
                i_at > j_at, own, jnp.where(i_at < j_at, opposite, own + opposite)
            )
            mixing.append((jnp.exp(gap) * amount * inner).astype(jnp.bfloat16))
        pieces = []
        for pair in range(per_group // 2):
            x_pair = x[:, pair * 2 * HEAD_DIM : (pair + 1) * 2 * HEAD_DIM]
            both = jnp.concatenate(
                [jnp.where(half_lane, x_pair, 0.0), jnp.where(half_lane, 0.0, x_pair)], axis=0
            ).astype(jnp.bfloat16)
            left = jnp.concatenate([mixing[2 * pair], mixing[2 * pair + 1]], axis=1)
            pieces.append(jnp.dot(left, both, preferred_element_type=jnp.float32))
        y_ref[at, :] = jnp.concatenate(pieces, axis=1)
        totals.append(total)
        columns_kept.append(cum_col)
    for first, order in ((0, range(blocks)), (1, range(blocks - 1, -1, -1))):
        lanes = slice(first * width, (first + 1) * width)
        held = jnp.zeros((STATE, width), jnp.float32)
        for block in order:
            entry_scr[block, :, lanes] = held.astype(jnp.bfloat16)
            factor = spread_heads(
                jnp.exp(totals[block][:, first * per_group : (first + 1) * per_group]), per_group
            )
            held = held * factor + parts[block][:, lanes]
        state_ref[first, 0, 0:STATE, :] = held.astype(jnp.bfloat16)
        whole = totals[0]
        for block in range(1, blocks):
            whole = whole + totals[block]
        whole = spread_heads(
            jnp.exp(whole[:, first * per_group : (first + 1) * per_group]), per_group
        )
        state_ref[first, 0, STATE:, :] = jnp.broadcast_to(
            whole, (state_ref.shape[2] - STATE, width)
        ).astype(jnp.bfloat16)
    for block in range(blocks):
        at = slice(block * BLOCK, (block + 1) * BLOCK)
        readout = jnp.dot(c_out[at, :], entry_scr[block], preferred_element_type=jnp.float32)
        fade_in = jnp.exp(columns_kept[block])
        y_ref[at, :] = (
            y_ref[at, :]
            + readout[:, :width] * spread_heads(fade_in[:, 0:per_group], per_group)
            + readout[:, width:] * spread_heads(fade_in[:, per_group:rows], per_group)
        )
        offset = jnp.zeros((1, rows), jnp.float32)
        for earlier in range(blocks):
            if earlier < block:
                offset = offset + jnp.where(col_at < per_group, totals[earlier], 0.0)
            if earlier > block:
                offset = offset + jnp.where(col_at < per_group, 0.0, totals[earlier])
        reach_ref[0, at, :] = jnp.exp(columns_kept[block] + offset)


def exchange_kernel(axis, source, target, send_sem, recv_sem):
    here, peers = lax.axis_index(axis), lax.axis_size(axis)
    barrier = pltpu.get_barrier_semaphore()
    for away in range(1, peers):
        pl.semaphore_signal(
            barrier, inc=1, device_id={axis: lax.rem(here + away, peers)}, device_id_type=MESH_IDS
        )
    pl.semaphore_wait(barrier, peers - 1)
    copies = []
    for away in range(1, peers):
        peer = lax.rem(here + away, peers)
        copies.append(
            pltpu.make_async_remote_copy(
                src_ref=source.at[jnp.where(peer > here, 0, 1)],
                dst_ref=target.at[here],
                send_sem=send_sem.at[away - 1],
                recv_sem=recv_sem.at[away - 1],
                device_id={axis: peer},
                device_id_type=MESH_IDS,
            )
        )
    for copy in copies:
        copy.start()
    target[here] = jnp.zeros(target.shape[1:], target.dtype)
    for copy in copies:
        copy.wait()


def blend_kernel(
    here_ref, y_ref, c_ref, reach_ref, states_ref, gate_ref, gain_ref, weight_ref, out_ref, carry_scr
):
    peers, groups, _, width = states_ref.shape
    per_group = width // HEAD_DIM
    rows = 2 * per_group

    @pl.when(pl.program_id(0) == 0)
    def _():
        here = here_ref[0]
        for group in range(groups):
            for first in range(2):
                held = jnp.zeros((STATE, width), jnp.float32)
                order = range(peers) if first == 0 else range(peers - 1, -1, -1)
                for peer in order:
                    fresh = states_ref[peer, group, 0:STATE, :].astype(jnp.float32)
                    factor = states_ref[peer, group, STATE : STATE + 1, :].astype(jnp.float32)
                    reached = peer < here if first == 0 else peer > here
                    held = jnp.where(reached, held * factor + fresh, held)
                carry_scr[group, :, first * width : (first + 1) * width] = held.astype(jnp.bfloat16)

    mixed = []
    for group in range(groups):
        lanes = slice(group * width, (group + 1) * width)
        c = c_ref[:, group * STATE : (group + 1) * STATE]
        readout = jnp.dot(c, carry_scr[group], preferred_element_type=jnp.float32)
        reach = reach_ref[group]
        y = (
            y_ref[:, lanes]
            + readout[:, :width] * spread_heads(reach[:, 0:per_group], per_group)
            + readout[:, width:] * spread_heads(reach[:, per_group:rows], per_group)
        )
        gated = y * silu(gate_ref[:, lanes].astype(jnp.float32))
        square = jnp.mean(gated * gated, axis=-1, keepdims=True)
        mixed.append((gated * lax.rsqrt(square + EPSILON) * gain_ref[:, lanes]).astype(jnp.bfloat16))
    rows_mixed = mixed[0] if groups == 1 else jnp.concatenate(mixed, axis=1)
    out_ref[...] = jnp.dot(
        rows_mixed, weight_ref[...], preferred_element_type=jnp.float32
    ).astype(jnp.bfloat16)


def mixer(
    result_switch_mapped, channel_feed_mapped, write_coefficient_mapped,
    emission_coefficient_mapped, channel_feed_taps, write_coefficient_taps,
    emission_coefficient_taps, raw_increments, channel_log_fade_speed, extra_log_fade,
    cluster_scaling_factor, blend_result_matrix,
):
    count, inner_here = channel_feed_mapped.shape
    groups = write_coefficient_mapped.shape[1] // STATE
    width = inner_here // groups
    per_group = width // HEAD_DIM
    rim = channel_feed_taps.shape[0] // 2
    sources = (channel_feed_mapped, write_coefficient_mapped, emission_coefficient_mapped)
    low = neighbour_rows(jnp.concatenate([s[-rim:] for s in sources], 1), "sp", 1)
    high = neighbour_rows(jnp.concatenate([s[:rim] for s in sources], 1), "sp", -1)
    cuts = (inner_here, inner_here + groups * STATE)
    lows, highs = jnp.split(low, cuts, axis=1), jnp.split(high, cuts, axis=1)
    step = jax.nn.softplus(raw_increments.astype(jnp.float32))
    fade = -step * jnp.exp(channel_log_fade_speed)[..., None] + extra_log_fade

    def by_group(value):
        value = value.reshape(2, groups, per_group, count)
        return jnp.transpose(value, (1, 0, 2, 3)).reshape(groups, 2 * per_group, count)

    fades = jnp.concatenate([by_group(fade), by_group(step)], axis=1)
    rows = 2 * per_group
    depth = STATE + 16

    def wide(height):
        return pl.BlockSpec((height, width), lambda g: (0, g))

    def narrow(height):
        return pl.BlockSpec((height, STATE), lambda g: (0, g))

    taps = channel_feed_taps.shape[0]
    y, c, states, reach = pl.pallas_call(
        sweep_kernel,
        grid=(groups,),
        in_specs=[
            wide(count), narrow(count), narrow(count), wide(rim), wide(rim), narrow(rim),
            narrow(rim), narrow(rim), narrow(rim), wide(taps), narrow(taps), narrow(taps),
            pl.BlockSpec((1, 2 * rows, count), lambda g: (g, 0, 0)),
        ],
        out_specs=[
            wide(count), narrow(count),
            pl.BlockSpec((2, 1, depth, width), lambda g: (0, g, 0, 0)),
            pl.BlockSpec((1, count, rows), lambda g: (g, 0, 0)),
        ],
        out_shape=[
            jax.ShapeDtypeStruct((count, inner_here), jnp.float32),
            jax.ShapeDtypeStruct((count, groups * STATE), jnp.bfloat16),
            jax.ShapeDtypeStruct((2, groups, depth, width), jnp.bfloat16),
            jax.ShapeDtypeStruct((groups, count, rows), jnp.float32),
        ],
        scratch_shapes=[
            pltpu.VMEM((count + 16, width), jnp.float32),
            pltpu.VMEM((count + 16, STATE), jnp.float32),
            pltpu.VMEM((count + 16, STATE), jnp.float32),
            pltpu.VMEM((count // BLOCK, STATE, 2 * width), jnp.bfloat16),
        ],
        cost_estimate=pl.CostEstimate(flops=200_000_000, bytes_accessed=4_000_000, transcendentals=0),
        name="sweep",
    )(
        *sources, lows[0], highs[0], lows[1], highs[1], lows[2], highs[2],
        channel_feed_taps, write_coefficient_taps, emission_coefficient_taps, fades,
    )
    peers = lax.axis_size("sp")
    gathered = pl.pallas_call(
        functools.partial(exchange_kernel, "sp"),
        in_specs=[pl.BlockSpec(memory_space=pltpu.VMEM)],
        out_specs=pl.BlockSpec(memory_space=pltpu.VMEM),
        out_shape=jax.ShapeDtypeStruct((peers,) + states.shape[1:], jnp.bfloat16),
        scratch_shapes=[
            pltpu.SemaphoreType.DMA((peers - 1,)),
            pltpu.SemaphoreType.DMA((peers - 1,)),
        ],
        compiler_params=pltpu.CompilerParams(collective_id=0, has_side_effects=True),
        name="exchange",
    )(states)
    features = blend_result_matrix.shape[1]
    here = jnp.full((1,), lax.axis_index("sp"), jnp.int32)
    return pl.pallas_call(
        blend_kernel,
        grid=(count // BLOCK,),
        in_specs=[
            pl.BlockSpec(memory_space=pltpu.SMEM),
            pl.BlockSpec((BLOCK, inner_here), lambda i: (i, 0)),
            pl.BlockSpec((BLOCK, groups * STATE), lambda i: (i, 0)),
            pl.BlockSpec((groups, BLOCK, rows), lambda i: (0, i, 0)),
            pl.BlockSpec(gathered.shape, lambda i: (0, 0, 0, 0)),
            pl.BlockSpec((BLOCK, inner_here), lambda i: (i, 0)),
            pl.BlockSpec((1, inner_here), lambda i: (0, 0)),
            pl.BlockSpec(blend_result_matrix.shape, lambda i: (0, 0)),
        ],
        out_specs=pl.BlockSpec((BLOCK, features), lambda i: (i, 0)),
        out_shape=jax.ShapeDtypeStruct((count, features), jnp.bfloat16),
        scratch_shapes=[pltpu.VMEM((groups, STATE, 2 * width), jnp.bfloat16)],
        name="blend",
    )(
        here, y, c, reach, gathered, result_switch_mapped,
        cluster_scaling_factor.reshape(1, -1), blend_result_matrix,
    )


def rms_scale(stream, gain):
    values = stream.astype(jnp.float32)
    return (
        values * lax.rsqrt(jnp.mean(values * values, axis=-1, keepdims=True) + EPSILON) * gain
    ).astype(jnp.bfloat16)


def per_device(
    skip_stream_entry,
    result_switch_mapped,
    channel_feed_mapped,
    write_coefficient_mapped,
    emission_coefficient_mapped,
    channel_feed_taps,
    write_coefficient_taps,
    emission_coefficient_taps,
    raw_increments,
    channel_log_fade_speed,
    extra_log_fade,
    cluster_scaling_factor,
    blend_result_matrix,
    routing_scaling_factor,
    specialist_switch_matrix,
    specialist_widen_matrix,
    specialist_contract_matrix,
    picked_specialists,
    router_affinities,
):
    partial = mixer(
        result_switch_mapped, channel_feed_mapped, write_coefficient_mapped,
        emission_coefficient_mapped, channel_feed_taps, write_coefficient_taps,
        emission_coefficient_taps, raw_increments, channel_log_fade_speed, extra_log_fade,
        cluster_scaling_factor, blend_result_matrix,
    )
    rows_here = skip_stream_entry.shape[0]
    projected = lax.psum_scatter(
        partial,
        "tp",
        scatter_dimension=0,
        tiled=True,
    ).astype(jnp.float32)
    after_mixer = (skip_stream_entry.astype(jnp.float32) + projected).astype(jnp.bfloat16)
    normed = rms_scale(after_mixer, routing_scaling_factor)
    experts_here = specialist_switch_matrix.shape[0]
    expert_count = experts_here * lax.axis_size("sp")
    capacity = max(2, 3 * TOP * rows_here // (2 * expert_count))
    peers = lax.axis_size("sp")
    slot_total = capacity * peers
    flat_routes = picked_specialists.reshape(-1)
    one_hot = (flat_routes[:, None] == jnp.arange(expert_count, dtype=jnp.int32)[None, :]).astype(
        jnp.int32
    )
    earlier_count = jnp.cumsum(one_hot, axis=0) - one_hot
    slot_rank = jnp.sum(earlier_count * one_hot, axis=1)
    position = (flat_routes // experts_here) * capacity + slot_rank
    matches, blocks = [], []
    for expert in range(experts_here):
        place = jnp.where(flat_routes % experts_here == expert, position, -1)
        match = (place[:, None] == jnp.arange(slot_total, dtype=jnp.int32)[None, :]).astype(
            jnp.bfloat16
        )
        token_match = jnp.sum(match.reshape(rows_here, TOP, slot_total), axis=1)
        buffer = jnp.einsum(
            "rs,rd->sd", token_match, normed, preferred_element_type=jnp.float32
        ).astype(jnp.bfloat16)
        received = lax.all_to_all(buffer, "sp", split_axis=0, concat_axis=0, tiled=True)
        matches.append(match)
        blocks.append(lax.all_gather(received, "tp", axis=0, tiled=True))
    picked = jnp.zeros((rows_here * TOP, WIDTH), jnp.float32)
    for expert in range(experts_here):
        gate_part = jnp.dot(
            blocks[expert], specialist_switch_matrix[expert], preferred_element_type=jnp.float32
        )
        up_part = jnp.dot(
            blocks[expert], specialist_widen_matrix[expert], preferred_element_type=jnp.float32
        )
        hidden = (jax.nn.silu(gate_part) * up_part).astype(jnp.bfloat16)
        expert_out = lax.psum_scatter(
            jnp.dot(
                hidden, specialist_contract_matrix[expert], preferred_element_type=jnp.float32
            ).astype(jnp.bfloat16),
            "tp",
            scatter_dimension=0,
            tiled=True,
        )
        returned = lax.all_to_all(expert_out, "sp", split_axis=0, concat_axis=0, tiled=True)
        picked = picked + jnp.dot(matches[expert], returned, preferred_element_type=jnp.float32)
    weights = router_affinities / jnp.sum(router_affinities, axis=-1, keepdims=True)
    mixture = jnp.sum(weights[..., None] * picked.reshape(rows_here, TOP, WIDTH), axis=1)
    return (after_mixer.astype(jnp.float32) + mixture).astype(jnp.bfloat16)


def solution(mesh):
    in_specs = (
        P(("sp", "tp"), None),
        P("sp", "tp"),
        P("sp", "tp"),
        P("sp", "tp"),
        P("sp", "tp"),
        P(None, "tp"),
        P(None, "tp"),
        P(None, "tp"),
        P(None, "tp", "sp"),
        P(None, "tp"),
        P(None, "tp", "sp"),
        P("tp"),
        P("tp", None),
        P(),
        P("sp", None, "tp"),
        P("sp", None, "tp"),
        P("sp", "tp", None),
        P(("sp", "tp"), None),
        P(("sp", "tp"), None),
    )
    out_specs = P(("sp", "tp"), None)
    return jax.shard_map(
        per_device, mesh=mesh, in_specs=in_specs, out_specs=out_specs, check_vma=False
    )
```

time: 441 us -> 277 us (0.63)
  local copies, waits for them, and re-layouts: 76.9 us -> 5.87 us
  other arithmetic: 57.6 us -> 5.64 us
  Pallas kernels: 0 us -> 32 us
  blocking collectives: 50.7 us -> 19.4 us
  matrix products: 50.2 us -> 28.9 us
  waiting for transfers between devices: 177 us -> 157 us
    all_gather x4 -> x0, blocking collectives: 38.7 us -> none  [prefix(): lax.all_gather(part.astype(kind), axis)]
    pallas_call x0 -> x3, Pallas kernels: none -> 32 us  [the longest x1 12.4 us: mixer(): pl.pallas_call(functools.partial(exchange_kernel, 'sp'), in_specs=[pl.Blo...]
    rev x6 -> x0, local copies, waits for them, and re-layouts: 25.5 us -> none  [the longest x1 9.4 us: blend_parts_list(): jnp.flip(inputs, 0)]
    dot_general x13 -> x8, matrix products: 50.2 us -> 28.9 us  [the longest x2 16.3 us: per_device(): jnp.dot(hidden, specialist_contract_matrix[expert], preferred_element_typ...]
    reshape x9 -> x8, local copies, waits for them, and re-layouts: 15.5 us -> 0.83 us  [the longest x1 0.62 us: per_device(): picked.reshape(rows_here, TOP, WIDTH)]
    mul x7 -> x0, other arithmetic: 14.2 us -> none  [the longest x3 9.7 us: centred_conv(): return jax.nn.silu(summed)]
    all_gather x1 -> x2, waiting for transfers between devices: 63.8 us -> 50.2 us  [per_device(): blocks.append(lax.all_gather(received, 'tp', axis=0, tiled=True))]
    slice x14 -> x2, local copies, waits for them, and re-layouts: 9.95 us -> 1.46 us  [mixer(): s[:rim]]
  transfers between devices with their start and end apart: 6 -> 9, of which waited for: 4 -> 6; matrix products, arithmetic and copies ran while one was open for 6% -> 12% of each run, Pallas kernels for 0% -> 0%
where the time goes in v1:
time: 277 us; the launch traced here: 276 us
  waiting for transfers between devices  157 us (57%)
  Pallas kernels  32 us (12%)
  matrix products  28.9 us (10%)
  blocking collectives  19.4 us (7%)
  starting transfers between devices  14.4 us (5%)
  between operations  13.4 us (5%)
  local copies, waits for them, and re-layouts  5.87 us (2%)
  other arithmetic  5.64 us (2%)
    reduce_scatter x2, waiting for transfers between devices, per_device(): lax.psum_scatter(jnp.dot(hidden, specialist_contract_matrix[expert], pref...  65.8 us
    all_gather x2, waiting for transfers between devices, per_device(): blocks.append(lax.all_gather(received, 'tp', axis=0, tiled=True))  50.2 us
    reduce_scatter x1, waiting for transfers between devices, per_device(): lax.psum_scatter(partial, 'tp', scatter_dimension=0, tiled=True)  35.1 us
    all_to_all x2, blocking collectives, per_device(): lax.all_to_all(buffer, 'sp', split_axis=0, concat_axis=0, tiled=True)  19.4 us
    dot_general x2, matrix products, per_device(): jnp.dot(hidden, specialist_contract_matrix[expert], preferred_element_typ...  16.3 us
    pallas_call x1, Pallas kernels, mixer(): pl.pallas_call(functools.partial(exchange_kernel, 'sp'), in_specs=[pl.Blo...  12.4 us
    dot_general x2, matrix products, per_device(): jnp.dot(blocks[expert], specialist_switch_matrix[expert], preferred_eleme...  11.2 us
    pallas_call x1, Pallas kernels, mixer(): pl.pallas_call(sweep_kernel, grid=(groups,), in_specs=[wide(count), narro...  11.1 us
  transfers between devices with their start and end apart: 9, of which 6 were waited for; matrix products, arithmetic and copies ran while one was open for 12% of the time, Pallas kernels for 0%

profile of v1, /device:TPU:0, one launch (start us, length us, event | category | flops | bytes accessed | tf_op | source)
XLA Modules:
  0.0 276.3 jit_solution(15918516790757223643)
XLA Ops:
  6.5 0.7 fusion.49
  7.3 0.7 fusion.50
  8.0 1.3 collective-permute-start.1
  9.3 5.5 %collective-permute-start = (bf16[2,1024]{1,0:T(2,128)(2,1)S(1)}, bf16[2,1024]{1,0:T(2,128)(2,1)S(1)}, u32[]{:S(2)}, u32[]{:S(2)}) collective-permute-start(bf16[2,1024]{1,0:T(2,128)(2,1)S(1)} %pad_maximum_fusion.1), channel_id=1, source_target_pairs={{0,8},{8,16},{16,24},{1,9},{9,17},{17,25},{2,10},{10,18},{18,26},{... | collective-permute-start | bytes 12296 | tf_op jit(solution)/shard_map/ppermute | solution.py:30
  14.8 0.7 exp.15
  15.5 0.8 multiply_add_fusion
  16.5 0.6 pad_maximum_fusion.fade_ref
  17.1 0.0 collective-permute-done
  17.1 0.6 fusion.53
  17.6 0.6 split.24.x_low
  18.2 0.0 collective-permute-done.1
  18.2 0.6 fusion.52
  18.8 0.6 split.25.x_high
  19.4 11.1 %sweep.1 = (f32[512,512]{1,0:T(8,128)}, bf16[512,256]{1,0:T(8,128)(2,1)}, bf16[2,2,144,256]{3,2,1,0:T(8,128)(2,1)}, f32[2,512,8]{2,1,0:T(8,128)}) custom-call(bf16[512,512]{1,0:T(8,128)(2,1)} %x_ref.1, bf16[512,256]{1,0:T(8,128)(2,1)} %b_ref.1, bf16[512,256]{1,0:T(8,128)(2,1)} %c_ref.1, bf16[2,512]{1,0:T(2,128)(2,1)} %split.24.x_low, ...), custom_call_target="tpu_custom_call" | custom-call | flops 200000000 | bytes 4000000 | tf_op jit(solution)/shard_map/sweep/pallas_call | solution.py:274
  30.5 12.4 %exchange.1.states_ref = bf16[4,2,144,256]{3,2,1,0:T(8,128)(2,1)} custom-call(bf16[2,2,144,256]{3,2,1,0:T(8,128)(2,1)} %get-tuple-element.12.source), custom_call_target="tpu_custom_call" | custom-call | tf_op jit(solution)/shard_map/exchange/pallas_call | solution.py:306
  42.9 0.0 copy-start.3
  42.9 0.0 copy-start
  43.0 8.5 %blend.1 = bf16[512,2048]{1,0:T(8,128)(2,1)} custom-call(s32[1]{0:T(128)} %bitcast.here_ref, f32[512,512]{1,0:T(8,128)} %get-tuple-element.9.y_ref, bf16[512,256]{1,0:T(8,128)(2,1)} %get-tuple-element.10.c_ref, f32[2,512,8]{2,1,0:T(8,128)} %get-tuple-element.11.reach_ref, bf16[4,2,144,256]{3,2,1,0:T(8,128)(2,1)} %exchange.1.states_ref, ...), custom_call_target="tpu_custom_call" | custom-call | tf_op jit(solution)/shard_map/blend/pallas_call | solution.py:320
  51.4 0.0 reduce-scatter.4.cloned.1.call-update
  51.5 0.0 all-gather.3.cloned.1.call-start
  51.5 0.0 copy-done.3
  51.5 0.1 copy.45
  51.6 0.1 reshape.140
  51.8 0.1 fusion.32
  51.8 0.2 reduce_window_sum.11
  52.0 0.2 select_reduce_fusion
  52.2 0.1 reduce_sum.64
  52.4 0.1 copy.50
  52.5 0.1 copy.53
  52.6 0.1 fusion.43
  52.7 35.1 %reduce-scatter.4.cloned.1.call-done = bf16[64,2048]{1,0:T(8,128)(2,1)} async-done(((bf16[512,2048]{1,0:T(8,128)(2,1)}), bf16[64,2048]{1,0:T(8,128)(2,1)}) %reduce-scatter.4.cloned.1.call-update) | async-done | bytes 262160 | tf_op jit(solution)/shard_map/reduce_scatter | solution.py:378
  87.8 1.1 fusion.26
  89.0 0.3 convolution_convert_fusion.3
  89.3 9.9 %all_to_all.48 = bf16[4,24,2048]{2,1,0:T(8,128)(2,1)} all-to-all(bf16[4,24,2048]{2,1,0:T(8,128)(2,1)S(1)} %bitcast.53), channel_id=1, replica_groups=mesh['sp'=4,'tp'=8] {'sp'}, dimensions={0} | all-to-all | bytes 786432 | tf_op jit(solution)/shard_map/all_to_all | solution.py:408
  99.2 0.0 all-gather.3.cloned.1.call-update
  99.2 0.0 all-gather.5.cloned.1.call-start
  99.3 0.1 copy.54
  99.3 0.1 fusion.42
  99.4 0.3 convolution_convert_fusion.2
  99.8 9.5 %all_to_all.49 = bf16[4,24,2048]{2,1,0:T(8,128)(2,1)} all-to-all(bf16[4,24,2048]{2,1,0:T(8,128)(2,1)S(1)} %bitcast.52), channel_id=1, replica_groups=mesh['sp'=4,'tp'=8] {'sp'}, dimensions={0} | all-to-all | bytes 786432 | tf_op jit(solution)/shard_map/all_to_all | solution.py:408
  109.3 0.0 all-gather.5.cloned.1.call-update
  109.3 0.0 reduce-scatter.6.cloned.1.call-start
  109.4 25.4 %all-gather.3.cloned.1.call-done = bf16[768,2048]{1,0:T(8,128)(2,1)} async-done(((bf16[96,2048]{1,0:T(8,128)(2,1)}), bf16[768,2048]{1,0:T(8,128)(2,1)}) %all-gather.3.cloned.1.call-update) | async-done | bytes 3145744 | tf_op jit(solution)/shard_map/all_gather | solution.py:410
  134.8 5.6 %fusion.8 = f32[768,512]{1,0:T(8,128)} fusion(bf16[768,2048]{1,0:T(8,128)(2,1)} %all-gather.3.cloned.1.call-done, bf16[2,2048,512]{2,1,0:T(8,128)(2,1)} %param.33), kind=kOutput, calls=%fused_computation.13 | convolution fusion | flops 1610612736 | bytes 6815744 | tf_op jit(solution)/shard_map/dot_general | solution.py:413
  140.4 8.1 %convolution_convert_fusion.1 = bf16[768,2048]{1,0:T(8,128)(2,1)} fusion(bf16[2,512,2048]{2,1,0:T(8,128)(2,1)} %param.35, f32[768,512]{1,0:T(8,128)} %fusion.8, bf16[768,2048]{1,0:T(8,128)(2,1)S(1)} %copy-done.4, bf16[2,2048,512]{2,1,0:T(8,128)(2,1)} %param.34), kind=kOutput, calls=%fused_computation.1 | convolution fusion | flops 3225157632 | bytes 12058624 | tf_op jit(solution)/shard_map/dot_general | solution.py:421
  148.5 0.0 reduce-scatter.6.cloned.1.call-update
  148.5 0.2 reduce-scatter.8.cloned.1.call-start
  148.8 24.8 %all-gather.5.cloned.1.call-done = bf16[768,2048]{1,0:T(8,128)(2,1)} async-done(((bf16[96,2048]{1,0:T(8,128)(2,1)}), bf16[768,2048]{1,0:T(8,128)(2,1)}) %all-gather.5.cloned.1.call-update) | async-done | bytes 3145744 | tf_op jit(solution)/shard_map/all_gather | solution.py:410
  173.6 5.6 %fusion.3 = f32[768,512]{1,0:T(8,128)} fusion(bf16[768,2048]{1,0:T(8,128)(2,1)} %all-gather.5.cloned.1.call-done, bf16[2,2048,512]{2,1,0:T(8,128)(2,1)} %param.33), kind=kOutput, calls=%fused_computation.8 | convolution fusion | flops 1610612736 | bytes 6815744 | tf_op jit(solution)/shard_map/dot_general | solution.py:413
  179.2 8.2 %convolution_convert_fusion = bf16[768,2048]{1,0:T(8,128)(2,1)} fusion(bf16[2,512,2048]{2,1,0:T(8,128)(2,1)} %param.35, f32[768,512]{1,0:T(8,128)} %fusion.3, bf16[768,2048]{1,0:T(8,128)(2,1)S(1)} %copy-done.5, bf16[2,2048,512]{2,1,0:T(8,128)(2,1)} %param.34), kind=kOutput, calls=%fused_computation | convolution fusion | flops 3225157632 | bytes 12058624 | tf_op jit(solution)/shard_map/dot_general | solution.py:421
  187.4 0.0 reduce-scatter.8.cloned.1.call-update
  187.4 27.6 %reduce-scatter.6.cloned.1.call-done = bf16[96,2048]{1,0:T(8,128)(2,1)} async-done(((bf16[768,2048]{1,0:T(8,128)(2,1)}), bf16[96,2048]{1,0:T(8,128)(2,1)}) %reduce-scatter.6.cloned.1.call-update) | async-done | bytes 393232 | tf_op jit(solution)/shard_map/reduce_scatter | solution.py:420
  215.0 3.6 %all-to-all-start.1 = ((bf16[4,24,2048]{2,1,0:T(8,128)(2,1)}), bf16[4,24,2048]{2,1,0:T(8,128)(2,1)S(1)}, u32[]{:S(2)}, u32[]{:S(2)}) async-start(bf16[4,24,2048]{2,1,0:T(8,128)(2,1)} %bitcast.56), calls=%async_computation.3 | async-start | bytes 786432 | tf_op jit(solution)/shard_map/all_to_all | solution.py:428
  218.7 0.0 copy-done.2
  218.7 38.2 %reduce-scatter.8.cloned.1.call-done = bf16[96,2048]{1,0:T(8,128)(2,1)} async-done(((bf16[768,2048]{1,0:T(8,128)(2,1)}), bf16[96,2048]{1,0:T(8,128)(2,1)}) %reduce-scatter.8.cloned.1.call-update) | async-done | bytes 393232 | tf_op jit(solution)/shard_map/reduce_scatter | solution.py:420
  256.9 0.0 all-to-all-done.1
  256.9 3.6 %all-to-all-start.3 = ((bf16[4,24,2048]{2,1,0:T(8,128)(2,1)}), bf16[4,24,2048]{2,1,0:T(8,128)(2,1)S(1)}, u32[]{:S(2)}, u32[]{:S(2)}) async-start(bf16[4,24,2048]{2,1,0:T(8,128)(2,1)} %bitcast.57), calls=%async_computation.6 | async-start | bytes 786432 | tf_op jit(solution)/shard_map/all_to_all | solution.py:428
  260.6 0.1 copy.44
  260.7 0.3 fusion.33
  261.0 5.4 %all-to-all-done.3 = bf16[4,24,2048]{2,1,0:T(8,128)(2,1)S(1)} async-done(((bf16[4,24,2048]{2,1,0:T(8,128)(2,1)}), bf16[4,24,2048]{2,1,0:T(8,128)(2,1)S(1)}, u32[]{:S(2)}, u32[]{:S(2)}) %all-to-all-start.3) | async-done | bytes 393248 | tf_op jit(solution)/shard_map/all_to_all | solution.py:428
  266.5 0.3 convolution_add_fusion
  266.8 0.6 reshape.141
  267.5 1.5 multiply_reduce_fusion
  269.0 0.8 fusion.29
  (24 shorter events, 0.2 us)
Async XLA Ops:
  6.5 81.2 %reduce-scatter.4.cloned.1.call-start = ((), (), s32[]{:S(2)}) async-start(), calls=%async_computation.7 | async-start | bytes 2359296 | tf_op jit(solution)/shard_map/reduce_scatter | solution.py:378
  8.0 10.2 %collective-permute-start.1 = (bf16[2,1024]{1,0:T(2,128)(2,1)S(1)}, bf16[2,1024]{1,0:T(2,128)(2,1)S(1)}, u32[]{:S(2)}, u32[]{:S(2)}) collective-permute-start(bf16[2,1024]{1,0:T(2,128)(2,1)S(1)} %pad_maximum_fusion.2), channel_id=1, source_target_pairs={{8,0},{16,8},{24,16},{9,1},{17,9},{25,17},{10,2},{18,10},{26,18},{... | collective-permute-start | bytes 12296 | tf_op jit(solution)/shard_map/ppermute | solution.py:30
  9.3 7.8 %collective-permute-start = (bf16[2,1024]{1,0:T(2,128)(2,1)S(1)}, bf16[2,1024]{1,0:T(2,128)(2,1)S(1)}, u32[]{:S(2)}, u32[]{:S(2)}) collective-permute-start(bf16[2,1024]{1,0:T(2,128)(2,1)S(1)} %pad_maximum_fusion.1), channel_id=1, source_target_pairs={{0,8},{8,16},{16,24},{1,9},{9,17},{17,25},{2,10},{10,18},{18,26},{... | collective-permute-start | bytes 12296 | tf_op jit(solution)/shard_map/ppermute | solution.py:30
  42.9 8.6 %copy-start.3 = (s32[64,2]{0,1:T(2,128)S(1)}, s32[64,2]{0,1:T(2,128)}, u32[]{:S(2)}) copy-start(s32[64,2]{0,1:T(2,128)} %param.36) | copy-start | bytes 1540
  42.9 44.8 %copy-start = (bf16[64,2048]{1,0:T(8,128)(2,1)S(1)}, bf16[64,2048]{1,0:T(8,128)(2,1)}, u32[]{:S(2)}) copy-start(bf16[64,2048]{1,0:T(8,128)(2,1)} %param.19) | copy-start | bytes 786436
  51.4 37.5 %copy-start.1 = (f32[2048]{0:T(1024)S(1)}, f32[2048]{0:T(1024)}, u32[]{:S(2)}) copy-start(f32[2048]{0:T(1024)} %param.32) | copy-start | bytes 24580
  51.5 83.3 %all-gather.3.cloned.1.call-start = ((), (), s32[]{:S(2)}) async-start(), calls=%async_computation.8 | async-start | bytes 3538944 | tf_op jit(solution)/shard_map/all_gather | solution.py:410
  99.2 74.3 %all-gather.5.cloned.1.call-start = ((), (), s32[]{:S(2)}) async-start(), calls=%async_computation.10 | async-start | bytes 3538944 | tf_op jit(solution)/shard_map/all_gather | solution.py:410
  109.3 105.7 %reduce-scatter.6.cloned.1.call-start = ((), (), s32[]{:S(2)}) async-start(), calls=%async_computation.9 | async-start | bytes 3538944 | tf_op jit(solution)/shard_map/reduce_scatter | solution.py:420
  134.8 5.6 %copy-start.4 = (bf16[768,2048]{1,0:T(8,128)(2,1)S(1)}, bf16[768,2048]{1,0:T(8,128)(2,1)}, u32[]{:S(2)}) copy-start(bf16[768,2048]{1,0:T(8,128)(2,1)} %all-gather.3.cloned.1.call-done) | copy-start | bytes 9437188
  148.5 108.4 %reduce-scatter.8.cloned.1.call-start = ((), (), s32[]{:S(2)}) async-start(), calls=%async_computation.11 | async-start | bytes 3538944 | tf_op jit(solution)/shard_map/reduce_scatter | solution.py:420
  173.6 5.6 %copy-start.5 = (bf16[768,2048]{1,0:T(8,128)(2,1)S(1)}, bf16[768,2048]{1,0:T(8,128)(2,1)}, u32[]{:S(2)}) copy-start(bf16[768,2048]{1,0:T(8,128)(2,1)} %all-gather.5.cloned.1.call-done) | copy-start | bytes 9437188
  187.4 31.3 %copy-start.2 = (f32[64,2]{0,1:T(2,128)S(1)}, f32[64,2]{0,1:T(2,128)}, u32[]{:S(2)}) copy-start(f32[64,2]{0,1:T(2,128)} %param.37) | copy-start | bytes 1540
  215.0 41.9 %all-to-all-start.1 = ((bf16[4,24,2048]{2,1,0:T(8,128)(2,1)}), bf16[4,24,2048]{2,1,0:T(8,128)(2,1)S(1)}, u32[]{:S(2)}, u32[]{:S(2)}) async-start(bf16[4,24,2048]{2,1,0:T(8,128)(2,1)} %bitcast.56), calls=%async_computation.3 | async-start | bytes 786432 | tf_op jit(solution)/shard_map/all_to_all | solution.py:428
  256.9 9.5 %all-to-all-start.3 = ((bf16[4,24,2048]{2,1,0:T(8,128)(2,1)}), bf16[4,24,2048]{2,1,0:T(8,128)(2,1)S(1)}, u32[]{:S(2)}, u32[]{:S(2)}) async-start(bf16[4,24,2048]{2,1,0:T(8,128)(2,1)} %bitcast.57), calls=%async_computation.6 | async-start | bytes 786432 | tf_op jit(solution)/shard_map/all_to_all | solution.py:428
Sparse Core Ops, SparseCore 0:
  51.6 36.1 reduce-scatter.3
  99.3 35.3 all-gather.2
  136.4 37.1 all-gather.4
  175.7 39.2 reduce-scatter.5
  217.2 39.7 reduce-scatter.7
